TPU v7x, 32 devices: a whole 2x2x4 slice. The times are simulated.
32 devices in a mesh: grp: 2 (over y), sp: 4 (over z), tp: 4 (over x, core).
Axes of the slice: x: 2, y: 2, z: 4, core: 2. Of those that a mesh axis runs over, the one named last changes fastest.
Arguments:
- stream: bfloat16 [12288, 4096], P(('grp', 'sp', 'tp')), parts along dimension 0, may hold values from -6 to 6
- norm_gain: float32 [2, 4096], replicated, may hold values from 0.1 to 1.9
- mix_weight: bfloat16 [2, 4, 1024, 1024], P(None, None, 'sp', 'tp'), may hold values from -0.1875 to 0.1875
- branch_scale: float32 [2, 4096], replicated, may hold values from 0.1 to 1.9
Outputs:
- result: bfloat16 [12288, 4096], P(('grp', 'sp', 'tp')), parts along dimension 0
There are 2 independent parts, one for each index of `grp`. A program takes and returns all parts, laid end to end along the dimension named above; an argument that names none is the same for every part. Nothing has to cross between parts.
All inputs are finite; a program needn't handle non-finite values.
Results may differ from a plain program's by a relative error of at most 0.0056.
Values may be sent and summed in bfloat16 or wider, within the bound.
A program may use at most 128 MiB of HBM per device.

v0:
```python
import jax
import jax.numpy as jnp
from jax import lax
from jax.sharding import PartitionSpec as P

GW = 1024
G = 4
LAYERS = 2
epsilon = 1e-06
window_lengths = (2, 4, 8, 16)
halo_rows = 15


def from_behind(block, axis, distance):
    devices = range(lax.axis_size(axis))
    route = [(i - distance, i) for i in devices if i - distance in devices]
    return lax.ppermute(block, axis, route)


def per_device(stream, norm_gain, mix_weight, branch_scale):
    row_count = stream.shape[0]
    feature_width = stream.shape[1]
    offset = lax.axis_index(("sp", "tp")) * row_count
    counts_base = (offset + lax.iota(jnp.int32, row_count)).astype(jnp.float32) + 1.0
    residual = stream.astype(jnp.float32)
    for layer_idx in range(LAYERS):
        scale_rows = lax.rsqrt(jnp.mean(residual * residual, axis=1, keepdims=True) + epsilon)
        normed = (residual * scale_rows * norm_gain[layer_idx]).astype(jnp.bfloat16)
        earlier = from_behind(normed[row_count - halo_rows :], ("sp", "tp"), 1)
        extended = jnp.concatenate([earlier, normed], axis=0).astype(jnp.float32)
        pieces = []
        for group_idx in range(G):
            window_len = window_lengths[group_idx]
            segment = extended[:, group_idx * GW : (group_idx + 1) * GW]
            own_rows = segment[halo_rows:]
            running = own_rows
            for back_step in range(1, window_len):
                running = (
                    running + segment[halo_rows - back_step : halo_rows - back_step + row_count]
                )
            window_mean = running / jnp.minimum(counts_base, float(window_len))[:, None]
            pieces.append((window_mean - own_rows).astype(jnp.bfloat16))
        pooled = jnp.stack(pieces, axis=1)
        weight_shard = mix_weight[layer_idx]
        full_rows = lax.all_gather(weight_shard, "sp", axis=1, tiled=True)
        mixed_out = jnp.einsum(
            "rgc,gcn->rgn",
            pooled,
            lax.all_gather(full_rows, "tp", axis=2, tiled=True),
            preferred_element_type=jnp.float32,
        )
        residual = residual + mixed_out.reshape(row_count, feature_width) * branch_scale[layer_idx]
    return residual.astype(jnp.bfloat16)


def solution(mesh):
    return jax.shard_map(
        per_device,
        mesh=mesh,
        in_specs=(P(("grp", "sp", "tp"), None), P(), P(None, None, "sp", "tp"), P()),
        out_specs=P(("grp", "sp", "tp"), None),
        check_vma=False,
    )
```

profile of v0, /device:TPU:9, one launch (start us, length us, event | category | flops | bytes accessed | tf_op | source)
XLA Modules:
  0.0 248.3 jit_solution(16958773101239605890)
XLA Ops:
  6.5 0.0 all-gather.9.cloned.1.call-start
  6.5 2.2 fusion.69
  8.8 0.0 copy-start.1
  8.8 0.0 all-gather.9.cloned.1.call-update
  8.8 0.0 all-gather.13.cloned.1.call-start
  8.9 0.7 all-gather.13.cloned.1.call-update
  9.6 0.0 all-gather.11.cloned.1.call-start
  9.6 44.4 %all-gather.9.cloned.1.call-done = bf16[1,4,1024,256]{3,2,1,0:T(8,128)(2,1)} async-done(((bf16[1,4,256,256]{3,2,1,0:T(8,128)(2,1)}), bf16[1,4,1024,256]{3,2,1,0:T(8,128)(2,1)}) %all-gather.9.cloned.1.call-update) | async-done | bytes 2097168 | tf_op jit(solution)/shard_map/all_gather | solution.py:45
  54.0 0.0 all-gather.11.cloned.1.call-update
  54.0 0.0 all-gather.15.cloned.1.call-start
  54.0 0.0 copy-done.1
  54.0 0.7 fusion.4
  54.7 0.0 copy-start.3
  54.8 45.3 %all-gather.13.cloned.1.call-done = bf16[1,4,1024,256]{3,2,1,0:T(8,128)(2,1)} async-done(((bf16[1,4,256,256]{3,2,1,0:T(8,128)(2,1)}), bf16[1,4,1024,256]{3,2,1,0:T(8,128)(2,1)}) %all-gather.13.cloned.1.call-update) | async-done | bytes 2097168 | tf_op jit(solution)/shard_map/all_gather | solution.py:45
  100.0 0.0 all-gather.15.cloned.1.call-update
  100.0 0.0 copy-done.3
  100.1 0.0 copy-start.4
  100.1 1.0 fusion.6
  101.1 0.0 copy-start.2
  101.1 1.7 copy-done.2
  102.8 4.2 %collective-permute-start = (bf16[15,4096]{1,0:T(8,128)(2,1)S(1)}, bf16[15,4096]{1,0:T(8,128)(2,1)S(1)}, u32[]{:S(2)}, u32[]{:S(2)}) collective-permute-start(bf16[15,4096]{1,0:T(8,128)(2,1)S(1)} %slice.340), channel_id=1, source_target_pairs={{0,1},{1,2},{2,3},{3,4},{4,5},{5,6},{6,7},{7,8},{8,9},{9,10},{10,1... | collective-permute-start | bytes 368648 | tf_op jit(solution)/shard_map/ppermute | solution.py:17
  107.0 0.0 copy-done.4
  107.1 1.8 collective-permute-done
  108.9 3.2 %maximum_convert_fusion = f32[399,4096]{1,0:T(8,128)S(1)} fusion(bf16[384,4096]{1,0:T(8,128)(2,1)} %copy-done.2, bf16[15,4096]{1,0:T(8,128)(2,1)S(1)} %collective-permute-done), kind=kLoop, calls=%fused_computation.13 | loop fusion | flops 6537216 | bytes 9805824 | tf_op jit(solution)/shard_map/convert_element_type | solution.py:30
  112.2 3.3 %fusion.62 = bf16[384,1,1024]{2,0,1:T(8,128)(2,1)} fusion(f32[384]{0:T(512)S(1)} %fusion.63, f32[399,4096]{1,0:T(8,128)S(1)} %maximum_convert_fusion), kind=kLoop, calls=%fused_computation.114 | loop fusion | flops 7077888 | bytes 25953792 | tf_op jit(solution)/shard_map/stack | solution.py:43
  115.4 3.6 %fusion.56 = (bf16[384,1,1024]{2,0,1:T(8,128)(2,1)}, bf16[384,1,1024]{2,0,1:T(8,128)(2,1)}, bf16[384,1,1024]{2,0,1:T(8,128)(2,1)}) fusion(f32[384]{0:T(512)S(1)} %fusion.66, f32[399,4096]{1,0:T(8,128)S(1)} %maximum_convert_fusion, f32[384]{0:T(512)S(1)} %get-tuple-element.18, f32[384]{0:T(512)S(1)} %get-tuple-element.17), kind=kLoop, calls=%fused_computation.108 | loop fusion | flops 7864320 | bytes 24384000 | tf_op jit(solution)/shard_map/stack | solution.py:43
  119.0 43.0 %all-gather.11.cloned.1.call-done = bf16[1,4,1024,1024]{3,2,1,0:T(8,128)(2,1)} async-done(((bf16[1,4,1024,256]{3,2,1,0:T(8,128)(2,1)}), bf16[1,4,1024,1024]{3,2,1,0:T(8,128)(2,1)}) %all-gather.11.cloned.1.call-update) | async-done | bytes 8388624 | tf_op jit(solution)/shard_map/all_gather | solution.py:49
  162.0 7.8 %fusion.21 = f32[4,48,8,1024]{3,2,1,0:T(8,128)S(1)} fusion(bf16[1,4,1024,1024]{3,2,1,0:T(8,128)(2,1)} %all-gather.11.cloned.1.call-done, bf16[384,1,1024]{2,0,1:T(8,128)(2,1)} %fusion.62, bf16[384,1,1024]{2,0,1:T(8,128)(2,1)} %get-tuple-element.10, bf16[384,1,1024]{2,0,1:T(8,128)(2,1)} %get-tuple-element.9, bf16[384,1,1024]{2,0,1:T(8,128)(2,1)} %get-tuple-element.8), kind=kOutput, calls=%fused_computation.29 | convolution fusion | flops 3225944064 | bytes 17825792 | tf_op jit(solution)/shard_map/rgc,gcn->rgn/dot_general | solution.py:46
  169.8 0.6 copy.7
  170.4 0.0 copy-start
  170.4 1.2 multiply_reduce_fusion
  171.6 2.0 copy-done
  173.7 1.6 multiply_convert_fusion
  175.3 2.3 collective-permute-start.1
  177.6 4.6 %collective-permute-done.1 = bf16[15,4096]{1,0:T(8,128)(2,1)S(1)} collective-permute-done((bf16[15,4096]{1,0:T(8,128)(2,1)S(1)}, bf16[15,4096]{1,0:T(8,128)(2,1)S(1)}, u32[]{:S(2)}, u32[]{:S(2)}) %collective-permute-start.1) | collective-permute-done | bytes 122912 | tf_op jit(solution)/shard_map/ppermute | solution.py:17
  182.2 0.9 maximum_convert_fusion.1
  183.1 3.3 %fusion.61 = bf16[384,1,1024]{2,0,1:T(8,128)(2,1)} fusion(f32[384]{0:T(512)S(1)} %fusion.63, f32[399,4096]{1,0:T(8,128)S(1)} %maximum_convert_fusion.1), kind=kLoop, calls=%fused_computation.113 | loop fusion | flops 7077888 | bytes 25953792 | tf_op jit(solution)/shard_map/stack | solution.py:43
  186.4 3.5 %fusion.55 = (bf16[384,1,1024]{2,0,1:T(8,128)(2,1)}, bf16[384,1,1024]{2,0,1:T(8,128)(2,1)}, bf16[384,1,1024]{2,0,1:T(8,128)(2,1)}) fusion(f32[384]{0:T(512)S(1)} %fusion.66, f32[399,4096]{1,0:T(8,128)S(1)} %maximum_convert_fusion.1, f32[384]{0:T(512)S(1)} %get-tuple-element.18, f32[384]{0:T(512)S(1)} %get-tuple-element.17), kind=kLoop, calls=%fused_computation.107 | loop fusion | flops 7864320 | bytes 24384000 | tf_op jit(solution)/shard_map/stack | solution.py:43
  189.9 34.3 %all-gather.15.cloned.1.call-done = bf16[1,4,1024,1024]{3,2,1,0:T(8,128)(2,1)} async-done(((bf16[1,4,1024,256]{3,2,1,0:T(8,128)(2,1)}), bf16[1,4,1024,1024]{3,2,1,0:T(8,128)(2,1)}) %all-gather.15.cloned.1.call-update) | async-done | bytes 8388624 | tf_op jit(solution)/shard_map/all_gather | solution.py:49
  224.3 0.0 slice-start
  224.3 0.0 slice-start.1
  224.3 7.9 %fusion.26 = f32[4,48,8,1024]{3,2,1,0:T(8,128)S(1)} fusion(bf16[1,4,1024,1024]{3,2,1,0:T(8,128)(2,1)} %all-gather.15.cloned.1.call-done, bf16[384,1,1024]{2,0,1:T(8,128)(2,1)} %fusion.61, bf16[384,1,1024]{2,0,1:T(8,128)(2,1)} %get-tuple-element.7, bf16[384,1,1024]{2,0,1:T(8,128)(2,1)} %get-tuple-element.6, bf16[384,1,1024]{2,0,1:T(8,128)(2,1)} %get-tuple-element.5), kind=kOutput, calls=%fused_computation.30 | convolution fusion | flops 3225944064 | bytes 17825792 | tf_op jit(solution)/shard_map/rgc,gcn->rgn/dot_general | solution.py:46
  232.2 3.4 %copy.8 = f32[4,48,8,1024]{3,2,0,1:T(8,128)} copy(f32[4,48,8,1024]{3,2,1,0:T(8,128)S(1)} %fusion.26) | data formatting | bytes 12582912 | tf_op jit(solution)/shard_map/reshape | solution.py:52
  235.6 0.0 slice-done
  235.6 0.0 slice-done.1
  235.6 6.2 %add_convert_fusion = bf16[384,4096]{1,0:T(8,128)(2,1)} fusion(f32[384,4096]{1,0:T(8,128)} %bitcast.43, f32[4096]{0:T(1024)S(1)} %bitcast.47, f32[384,4096]{1,0:T(8,128)S(1)} %bitcast.42, f32[4096]{0:T(1024)S(1)} %bitcast.46, bf16[384,4096]{1,0:T(8,128)(2,1)S(1)} %copy-done.1), kind=kLoop, calls=%fused_computation.10 | loop fusion | flops 9437184 | bytes 18907136 | tf_op jit(solution)/shard_map/convert_element_type | solution.py:53
  (10 shorter events, 0.2 us)
Async XLA Ops:
  6.5 47.4 %all-gather.9.cloned.1.call-start = ((), (), s32[]{:S(2)}) async-start(), calls=%async_computation | async-start | bytes 2621440 | tf_op jit(solution)/shard_map/all_gather | solution.py:45
  8.8 45.3 %copy-start.1 = (bf16[384,4096]{1,0:T(8,128)(2,1)S(1)}, bf16[384,4096]{1,0:T(8,128)(2,1)}, u32[]{:S(2)}) copy-start(bf16[384,4096]{1,0:T(8,128)(2,1)} %param.4) | copy-start | bytes 9437188
  8.8 91.2 %all-gather.13.cloned.1.call-start = ((), (), s32[]{:S(2)}) async-start(), calls=%async_computation.2 | async-start | bytes 2621440 | tf_op jit(solution)/shard_map/all_gather | solution.py:45
  9.6 152.5 %all-gather.11.cloned.1.call-start = ((), (), s32[]{:S(2)}) async-start(), calls=%async_computation.1 | async-start | bytes 10485760 | tf_op jit(solution)/shard_map/all_gather | solution.py:49
  54.0 170.3 %all-gather.15.cloned.1.call-start = ((), (), s32[]{:S(2)}) async-start(), calls=%async_computation.3 | async-start | bytes 10485760 | tf_op jit(solution)/shard_map/all_gather | solution.py:49
  54.7 45.3 %copy-start.3 = (f32[2,4096]{1,0:T(2,128)S(1)}, f32[2,4096]{1,0:T(2,128)}, u32[]{:S(2)}) copy-start(f32[2,4096]{1,0:T(2,128)} %param.5) | copy-start | bytes 98308
  100.1 6.9 %copy-start.4 = (f32[2,4096]{1,0:T(2,128)S(1)}, f32[2,4096]{1,0:T(2,128)}, u32[]{:S(2)}) copy-start(f32[2,4096]{1,0:T(2,128)} %param.7) | copy-start | bytes 98308
  101.1 1.7 copy-start.2
  102.8 6.1 %collective-permute-start = (bf16[15,4096]{1,0:T(8,128)(2,1)S(1)}, bf16[15,4096]{1,0:T(8,128)(2,1)S(1)}, u32[]{:S(2)}, u32[]{:S(2)}) collective-permute-start(bf16[15,4096]{1,0:T(8,128)(2,1)S(1)} %slice.340), channel_id=1, source_target_pairs={{0,1},{1,2},{2,3},{3,4},{4,5},{5,6},{6,7},{7,8},{8,9},{9,10},{10,1... | collective-permute-start | bytes 368648 | tf_op jit(solution)/shard_map/ppermute | solution.py:17
  170.4 3.3 %copy-start = (f32[4,48,8,1024]{3,2,0,1:T(8,128)}, f32[4,48,8,1024]{3,2,0,1:T(8,128)S(1)}, u32[]{:S(2)}) copy-start(f32[4,48,8,1024]{3,2,0,1:T(8,128)S(1)} %copy.7) | copy-start | bytes 18874372
  175.3 6.9 %collective-permute-start.1 = (bf16[15,4096]{1,0:T(8,128)(2,1)S(1)}, bf16[15,4096]{1,0:T(8,128)(2,1)S(1)}, u32[]{:S(2)}, u32[]{:S(2)}) collective-permute-start(bf16[15,4096]{1,0:T(8,128)(2,1)S(1)} %slice.371), channel_id=1, source_target_pairs={{0,1},{1,2},{2,3},{3,4},{4,5},{5,6},{6,7},{7,8},{8,9},{9,10},{10,1... | collective-permute-start | bytes 368648 | tf_op jit(solution)/shard_map/ppermute | solution.py:17
  224.3 11.3 %slice-start = ((s8[6291456]{0:T(1024)(128)(4,1)}), s8[4194304]{0:T(1024)(128)(4,1)S(1)}, s32[]{:S(2)}) async-start(s8[6291456]{0:T(1024)(128)(4,1)} %bitcast.40), calls=%async_computation.4 | async-start | bytes 8388608
  224.3 11.3 %slice-start.1 = ((s8[6291456]{0:T(1024)(128)(4,1)}), s8[2097152]{0:T(1024)(128)(4,1)S(1)}, s32[]{:S(2)}) async-start(s8[6291456]{0:T(1024)(128)(4,1)} %bitcast.40), calls=%async_computation.5 | async-start | bytes 4194304
Sparse Core Ops, SparseCore 0:
  8.9 44.9 all-gather.8
  55.5 44.4 all-gather.12
  101.6 60.4 all-gather.10
  163.4 60.7 all-gather.14
where the time goes:
time: 249 us; the launch traced here: 248 us
  waiting for transfers between devices  174 us (70%)
  other arithmetic  28.5 us (11%)
  matrix products  15.6 us (6%)
  between operations  13.3 us (5%)
  local copies, waits for them, and re-layouts  10.1 us (4%)
  starting transfers between devices  6.56 us (3%)
    all_gather x2, waiting for transfers between devices, per_device(): full_rows = lax.all_gather(weight_shard, 'sp', axis=1, tiled=True)  89.6 us
    all_gather x2, waiting for transfers between devices, per_device(): lax.all_gather(full_rows, 'tp', axis=2, tiled=True)  77.3 us
    dot_general x2, matrix products, per_device(): jnp.einsum('rgc,gcn->rgn', pooled, lax.all_gather(full_rows, 'tp', axis=2...  15.6 us
    another operation x4, other arithmetic, per_device(): pooled = jnp.stack(pieces, axis=1)  13.6 us
    ppermute x2, waiting for transfers between devices, from_behind(): return lax.ppermute(block, axis, route)  6.48 us
    ppermute x2, starting transfers between devices, from_behind(): return lax.ppermute(block, axis, route)  6.44 us
    convert_element_type x1, other arithmetic, per_device(): return residual.astype(jnp.bfloat16)  6.2 us
  transfers between devices with their start and end apart: 6, of which 6 were waited for; matrix products, arithmetic and copies ran while one was open for 12% of the time, Pallas kernels for 0%

commit v1 on v0

--- a/solution.py
+++ b/solution.py
@@ -9,6 +9,33 @@
 epsilon = 1e-06
 window_lengths = (2, 4, 8, 16)
 halo_rows = 15
+
+
+def laid_out(blocks, dim):
+    lengths = list(blocks.shape[1:])
+    lengths[dim] *= blocks.shape[0]
+    return jnp.moveaxis(blocks, 0, dim).reshape(lengths)
+
+
+def on_each_block(x, axis, dim, apply, out_dim):
+    count, index, rows = (lax.axis_size(axis), lax.axis_index(axis), x.shape[dim])
+    right = [(i, (i + 1) % count) for i in range(count)]
+    backward = [(i, (i - 1) % count) for i in range(count)]
+    halfway = count // 2
+    parts = {}
+    from_left = from_right = x
+    for step in range(halfway + 1):
+        next_left = lax.ppermute(from_left, axis, right) if step < halfway else None
+        next_right = (
+            lax.ppermute(from_right, axis, backward) if step < count - halfway - 1 else None
+        )
+        parts[-step] = apply(from_left, (index - step) % count * rows)
+        if 0 < step < count - halfway:
+            parts[step] = apply(from_right, (index + step) % count * rows)
+        from_left, from_right = (next_left, next_right)
+    parts = jnp.stack([parts[k] for k in sorted(parts)])
+    parts = parts[(jnp.arange(count) - index + halfway) % count]
+    return laid_out(parts, out_dim)
 
 
 def from_behind(block, axis, distance):
@@ -43,11 +70,14 @@
         pooled = jnp.stack(pieces, axis=1)
         weight_shard = mix_weight[layer_idx]
         full_rows = lax.all_gather(weight_shard, "sp", axis=1, tiled=True)
-        mixed_out = jnp.einsum(
-            "rgc,gcn->rgn",
-            pooled,
-            lax.all_gather(full_rows, "tp", axis=2, tiled=True),
-            preferred_element_type=jnp.float32,
+        mixed_out = on_each_block(
+            full_rows,
+            "tp",
+            2,
+            lambda shard, offset_2: jnp.einsum(
+                "rgc,gcn->rgn", pooled, shard, preferred_element_type=jnp.float32
+            ),
+            2,
         )
         residual = residual + mixed_out.reshape(row_count, feature_width) * branch_scale[layer_idx]
     return residual.astype(jnp.bfloat16)

time: 249 us -> 262 us (1.052); the launches traced: 248 us -> 258 us
  waiting for transfers between devices: 174 us -> 113 us
  local copies, waits for them, and re-layouts: 10.1 us -> 52.8 us
  starting transfers between devices: 6.56 us -> 17.3 us
  other arithmetic: 28.5 us -> 39.2 us
  matrix products: 15.6 us -> 22.1 us
    all_gather x2 -> x0, waiting for transfers between devices: 77.3 us -> none  [per_device(): lax.all_gather(full_rows, 'tp', axis=2, tiled=True)]
    ppermute x0 -> x6, waiting for transfers between devices: none -> 77 us  [the longest x4 77 us: on_each_block(): next_left = lax.ppermute(from_left, axis, right) if step < halfway else None]
    all_gather x2, waiting for transfers between devices: 89.6 us -> 35.8 us  [per_device(): full_rows = lax.all_gather(weight_shard, 'sp', axis=1, tiled=True)]
    transpose x0 -> x2, local copies, waits for them, and re-layouts: none -> 18.9 us  [laid_out(): return jnp.moveaxis(blocks, 0, dim).reshape(lengths)]
    another operation x0 -> x2, local copies, waits for them, and re-layouts: none -> 16.5 us  [per_device(): mixed_out.reshape(row_count, feature_width) * branch_scale[layer_idx]]
    gather x0 -> x2, local copies, waits for them, and re-layouts: none -> 12.7 us  [on_each_block(): parts = parts[(jnp.arange(count) - index + halfway) % count]]
    ppermute x0 -> x6, starting transfers between devices: none -> 9.18 us  [the longest x4 9.12 us: on_each_block(): next_left = lax.ppermute(from_left, axis, right) if step < halfway else None]
    dot_general x2 -> x8, matrix products: 15.6 us -> 22.1 us  [per_device(): jnp.einsum('rgc,gcn->rgn', pooled, shard, preferred_element_type=jnp.floa...]
  transfers between devices with their start and end apart: 6 -> 10, of which waited for: 6 -> 5; matrix products, arithmetic and copies ran while one was open for 12% -> 28% of each run, Pallas kernels for 0% -> 0%
where the time goes in v1:
time: 262 us; the launch traced here: 258 us
  waiting for transfers between devices  113 us (43%)
  local copies, waits for them, and re-layouts  52.8 us (20%)
  other arithmetic  39.2 us (15%)
  matrix products  22.1 us (8%)
  starting transfers between devices  17.3 us (7%)
  between operations  13.7 us (5%)
    ppermute x4, waiting for transfers between devices, on_each_block(): next_left = lax.ppermute(from_left, axis, right) if step < halfway else None  77 us
    all_gather x2, waiting for transfers between devices, per_device(): full_rows = lax.all_gather(weight_shard, 'sp', axis=1, tiled=True)  35.8 us
    dot_general x8, matrix products, per_device(): jnp.einsum('rgc,gcn->rgn', pooled, shard, preferred_element_type=jnp.floa...  22.1 us
    transpose x2, local copies, waits for them, and re-layouts, laid_out(): return jnp.moveaxis(blocks, 0, dim).reshape(lengths)  18.9 us
    another operation x2, local copies, waits for them, and re-layouts, per_device(): mixed_out.reshape(row_count, feature_width) * branch_scale[layer_idx]  16.5 us
    gather x2, local copies, waits for them, and re-layouts, on_each_block(): parts = parts[(jnp.arange(count) - index + halfway) % count]  12.7 us
    another operation x4, other arithmetic, per_device(): pooled = jnp.stack(pieces, axis=1)  12.4 us
    ppermute x4, starting transfers between devices, on_each_block(): next_left = lax.ppermute(from_left, axis, right) if step < halfway else None  9.12 us
  transfers between devices with their start and end apart: 10, of which 5 were waited for; matrix products, arithmetic and copies ran while one was open for 28% of the time, Pallas kernels for 0%

profile of v1, /device:TPU:9, one launch (start us, length us, event | category | flops | bytes accessed | tf_op | source)
XLA Modules:
  0.0 258.0 jit_solution(574488837918457934)
XLA Ops:
  6.5 0.0 all-gather.5.cloned.1.call-start
  6.5 2.2 fusion.43
  8.8 0.0 copy-start.7
  8.8 0.0 all-gather.5.cloned.1.call-update
  8.8 0.0 all-gather.7.cloned.1.call-start
  8.9 2.7 %fusion = f32[384]{0:T(512)S(1)} fusion(bf16[384,4096]{1,0:T(8,128)(2,1)} %param.4), kind=kLoop, calls=%fused_computation.5 | loop fusion | flops 4718208 | bytes 3147264 | tf_op jit(solution)/shard_map/reduce_sum | solution.py:54
  11.6 0.0 copy-done.7
  11.6 0.0 copy-done.1
  11.7 0.0 copy-start.8
  11.7 1.0 fusion.2
  12.7 0.0 copy-start.2
  12.7 1.7 copy-done.2
  14.4 3.7 %collective-permute-start = (bf16[15,4096]{1,0:T(8,128)(2,1)S(1)}, bf16[15,4096]{1,0:T(8,128)(2,1)S(1)}, u32[]{:S(2)}, u32[]{:S(2)}) collective-permute-start(bf16[15,4096]{1,0:T(8,128)(2,1)S(1)} %slice.344), channel_id=1, source_target_pairs={{0,1},{1,2},{2,3},{3,4},{4,5},{5,6},{6,7},{7,8},{8,9},{9,10},{10,1... | collective-permute-start | bytes 368648 | tf_op jit(solution)/shard_map/ppermute | solution.py:44
  18.1 0.0 all-gather.7.cloned.1.call-update
  18.2 0.0 copy-done.8
  18.2 35.8 %all-gather.5.cloned.1.call-done = bf16[1,4,1024,256]{3,2,1,0:T(8,128)(2,1)} async-done(((bf16[1,4,256,256]{3,2,1,0:T(8,128)(2,1)}), bf16[1,4,1024,256]{3,2,1,0:T(8,128)(2,1)}) %all-gather.5.cloned.1.call-update) | async-done | bytes 2097168 | tf_op jit(solution)/shard_map/all_gather | solution.py:72
  54.0 3.0 %collective-permute-start.1 = (bf16[4,1024,256]{2,1,0:T(8,128)(2,1)}, bf16[4,1024,256]{2,1,0:T(8,128)(2,1)}, u32[]{:S(2)}, u32[]{:S(2)}) collective-permute-start(bf16[4,1024,256]{2,1,0:T(8,128)(2,1)} %bitcast.5), channel_id=1, source_target_pairs={{0,1},{1,2},{2,3},{3,0},{4,5},{5,6},{6,7},{7,4},{8,9},{9,10},{10,1... | collective-permute-start | bytes 6291464 | tf_op jit(solution)/shard_map/ppermute | solution.py:28
  57.0 0.0 collective-permute-done
  57.0 2.8 %maximum_convert_fusion = f32[399,4096]{1,0:T(8,128)S(1)} fusion(bf16[384,4096]{1,0:T(8,128)(2,1)} %copy-done.2, bf16[15,4096]{1,0:T(8,128)(2,1)S(1)} %collective-permute-done), kind=kLoop, calls=%fused_computation.13 | loop fusion | flops 6537216 | bytes 9805824 | tf_op jit(solution)/shard_map/convert_element_type | solution.py:57
  59.8 3.6 %fusion.28 = (bf16[384,1,1024]{2,0,1:T(8,128)(2,1)}, bf16[384,1,1024]{2,0,1:T(8,128)(2,1)}, bf16[384,1,1024]{2,0,1:T(8,128)(2,1)}) fusion(f32[384]{0:T(512)S(1)} %fusion.38, f32[399,4096]{1,0:T(8,128)S(1)} %maximum_convert_fusion, f32[384]{0:T(512)S(1)} %get-tuple-element.18, f32[384]{0:T(512)S(1)} %get-tuple-element.17), kind=kLoop, calls=%fused_computation.102 | loop fusion | flops 7864320 | bytes 24384000 | tf_op jit(solution)/shard_map/stack | solution.py:70
  63.4 0.0 collective-permute-start.3
  63.4 32.8 %collective-permute-done.1 = bf16[4,1024,256]{2,1,0:T(8,128)(2,1)} collective-permute-done((bf16[4,1024,256]{2,1,0:T(8,128)(2,1)}, bf16[4,1024,256]{2,1,0:T(8,128)(2,1)}, u32[]{:S(2)}, u32[]{:S(2)}) %collective-permute-start.1) | collective-permute-done | bytes 2097184 | tf_op jit(solution)/shard_map/ppermute | solution.py:28
  96.2 2.5 collective-permute-start.2
  98.6 3.3 %fusion.34 = bf16[384,1,1024]{2,0,1:T(8,128)(2,1)} fusion(f32[384]{0:T(512)S(1)} %fusion.35, f32[399,4096]{1,0:T(8,128)S(1)} %maximum_convert_fusion), kind=kLoop, calls=%fused_computation.108 | loop fusion | flops 7077888 | bytes 25953792 | tf_op jit(solution)/shard_map/stack | solution.py:70
  101.9 0.0 all-gather.7.cloned.1.call-done
  101.9 1.9 collective-permute-start.5
  103.8 0.0 copy-start.3
  103.8 3.6 %convolution_bitcast_fusion.5 = f32[1,384,4,256]{3,1,2,0:T(8,128)S(1)} fusion(bf16[1,4,1024,256]{3,2,1,0:T(8,128)(2,1)} %all-gather.5.cloned.1.call-done, bf16[384,1,1024]{2,0,1:T(8,128)(2,1)} %fusion.34, bf16[384,1,1024]{2,0,1:T(8,128)(2,1)} %get-tuple-element.10, bf16[384,1,1024]{2,0,1:T(8,128)(2,1)} %get-tuple-element.9, ...), kind=kOutput, calls=%fused_computation.98 | convolution fusion | flops 810024960 | bytes 6815744 | tf_op jit(solution)/shard_map/rgc,gcn->rgn/dot_general | solution.py:77
  107.5 0.0 copy-done.3
  107.5 0.0 copy-done.4
  107.5 0.0 copy-done.5
  107.5 0.0 copy-done.6
  107.5 3.4 %convolution_bitcast_fusion.6 = f32[1,384,4,256]{3,1,2,0:T(8,128)S(1)} fusion(bf16[4,1024,256]{2,1,0:T(8,128)(2,1)} %collective-permute-done.1, bf16[384,1,1024]{2,0,1:T(8,128)(2,1)S(1)} %copy-done.3, bf16[384,1,1024]{2,0,1:T(8,128)(2,1)S(1)} %copy-done.6, bf16[384,1,1024]{2,0,1:T(8,128)(2,1)S(1)} %copy-done.5, bf16[384,1,1024]{2,0,1:T(8,128)(2,1)S(1)} %copy-done.4), kind=kOutput, calls=%fused_computation.99 | convolution fusion | flops 810024960 | bytes 6815744 | tf_op jit(solution)/shard_map/rgc,gcn->rgn/dot_general | solution.py:77
  111.0 0.0 collective-permute-done.3
  111.0 3.4 %convolution_bitcast_fusion.4 = f32[1,384,4,256]{3,1,2,0:T(8,128)S(1)} fusion(bf16[4,1024,256]{2,1,0:T(8,128)(2,1)} %collective-permute-done.3, bf16[384,1,1024]{2,0,1:T(8,128)(2,1)S(1)} %copy-done.3, bf16[384,1,1024]{2,0,1:T(8,128)(2,1)S(1)} %copy-done.6, bf16[384,1,1024]{2,0,1:T(8,128)(2,1)S(1)} %copy-done.5, bf16[384,1,1024]{2,0,1:T(8,128)(2,1)S(1)} %copy-done.4), kind=kOutput, calls=%fused_computation.97 | convolution fusion | flops 810024960 | bytes 6815744 | tf_op jit(solution)/shard_map/rgc,gcn->rgn/dot_general | solution.py:77
  114.4 10.8 %collective-permute-done.2 = bf16[4,1024,256]{2,1,0:T(8,128)(2,1)} collective-permute-done((bf16[4,1024,256]{2,1,0:T(8,128)(2,1)}, bf16[4,1024,256]{2,1,0:T(8,128)(2,1)}, u32[]{:S(2)}, u32[]{:S(2)}) %collective-permute-start.2) | collective-permute-done | bytes 2097184 | tf_op jit(solution)/shard_map/ppermute | solution.py:28
  125.2 3.4 %convolution_bitcast_fusion.7 = f32[1,384,4,256]{3,1,2,0:T(8,128)S(1)} fusion(bf16[4,1024,256]{2,1,0:T(8,128)(2,1)} %collective-permute-done.2, bf16[384,1,1024]{2,0,1:T(8,128)(2,1)S(1)} %copy-done.3, bf16[384,1,1024]{2,0,1:T(8,128)(2,1)S(1)} %copy-done.6, bf16[384,1,1024]{2,0,1:T(8,128)(2,1)S(1)} %copy-done.5, bf16[384,1,1024]{2,0,1:T(8,128)(2,1)S(1)} %copy-done.4), kind=kOutput, calls=%fused_computation.100 | convolution fusion | flops 810024960 | bytes 6815744 | tf_op jit(solution)/shard_map/rgc,gcn->rgn/dot_general | solution.py:77
  128.6 2.8 %pad_maximum_fusion = f32[4,384,4,256]{3,1,2,0:T(8,128)} fusion(f32[1,384,4,256]{3,1,2,0:T(8,128)S(1)} %convolution_bitcast_fusion.4, f32[1,384,4,256]{3,1,2,0:T(8,128)S(1)} %convolution_bitcast_fusion.5, f32[1,384,4,256]{3,1,2,0:T(8,128)S(1)} %convolution_bitcast_fusion.6, f32[1,384,4,256]{3,1,2,0:T(8,128)S(1)} %convolution_bitcast_fusion.7), kind=kLoop, calls=%fused_computation.8 | loop fusion | flops 4718592 | bytes 12582912 | tf_op jit(solution)/shard_map/stack | solution.py:36
  131.5 6.4 %gather_fusion = f32[4,384,4,256]{3,1,2,0:T(8,128)} fusion(f32[4,384,4,256]{3,1,2,0:T(8,128)} %pad_maximum_fusion, s32[1024]{0:T(1024)S(1)} %pad_clamp_fusion), kind=kCustom, calls=%fused_computation | custom fusion | bytes 12582928 | tf_op jit(solution)/shard_map/gather | solution.py:37
  137.9 9.4 %copy.5 = f32[384,4,4,256]{3,2,1,0:T(4,128)} copy(f32[384,4,4,256]{3,0,1,2:T(8,128)} %bitcast.69) | data formatting | bytes 12582912 | tf_op jit(solution)/shard_map/transpose | solution.py:17
  147.3 8.3 %reshape_reshape.6 = f32[384,4096]{1,0:T(8,128)} reshape(f32[384,4,4,256]{3,2,1,0:T(4,128)} %copy.5) | data formatting | bytes 12582912 | tf_op jit(solution)/shard_map/reshape;reshape | solution.py:82
  155.6 4.0 %multiply_reduce_fusion = f32[384]{0:T(512)S(1)} fusion(f32[384,4096]{1,0:T(8,128)} %reshape_reshape.6, f32[4096]{0:T(1024)S(1)} %bitcast.70, bf16[384,4096]{1,0:T(8,128)(2,1)S(1)} %copy-done.1), kind=kLoop, calls=%fused_computation.12 | loop fusion | flops 7863936 | bytes 9455104 | tf_op jit(solution)/shard_map/reduce_sum | solution.py:54
  159.6 0.6 copy-done
  160.2 1.6 multiply_convert_fusion
  161.8 4.4 %collective-permute-start.4 = (bf16[15,4096]{1,0:T(8,128)(2,1)S(1)}, bf16[15,4096]{1,0:T(8,128)(2,1)S(1)}, u32[]{:S(2)}, u32[]{:S(2)}) collective-permute-start(bf16[15,4096]{1,0:T(8,128)(2,1)S(1)} %slice.375), channel_id=1, source_target_pairs={{0,1},{1,2},{2,3},{3,4},{4,5},{5,6},{6,7},{7,8},{8,9},{9,10},{10,1... | collective-permute-start | bytes 368648 | tf_op jit(solution)/shard_map/ppermute | solution.py:44
  166.2 0.0 copy-done.9
  166.2 0.1 collective-permute-start.7
  166.2 0.0 collective-permute-done.5
  166.2 1.7 collective-permute-start.6
  168.0 0.1 collective-permute-done.4
  168.1 0.9 maximum_convert_fusion.1
  169.0 3.0 %fusion.27 = (bf16[384,1,1024]{2,0,1:T(8,128)(2,1)S(1)}, bf16[384,1,1024]{2,0,1:T(8,128)(2,1)S(1)}, bf16[384,1,1024]{2,0,1:T(8,128)(2,1)S(1)}) fusion(f32[384]{0:T(512)S(1)} %fusion.38, f32[399,4096]{1,0:T(8,128)S(1)} %maximum_convert_fusion.1, f32[384]{0:T(512)S(1)} %get-tuple-element.18, f32[384]{0:T(512)S(1)} %get-tuple-element.17), kind=kLoop, calls=%fused_computation.101 | loop fusion | flops 7864320 | bytes 24384000 | tf_op jit(solution)/shard_map/stack | solution.py:70
  172.0 2.5 fusion.33
  174.5 3.4 %convolution_bitcast_fusion.2 = f32[1,384,4,256]{3,1,2,0:T(8,128)S(1)} fusion(bf16[4,1024,256]{2,1,0:T(8,128)(2,1)} %collective-permute-done.5, bf16[384,1,1024]{2,0,1:T(8,128)(2,1)S(1)} %fusion.33, bf16[384,1,1024]{2,0,1:T(8,128)(2,1)S(1)} %get-tuple-element.7, bf16[384,1,1024]{2,0,1:T(8,128)(2,1)S(1)} %get-tuple-element.6, ...), kind=kOutput, calls=%fused_computation.95 | convolution fusion | flops 810024960 | bytes 6815744 | tf_op jit(solution)/shard_map/rgc,gcn->rgn/dot_general | solution.py:77
  178.0 1.6 convolution_bitcast_fusion.1
  179.6 33.5 %collective-permute-done.6 = bf16[4,1024,256]{2,1,0:T(8,128)(2,1)S(1)} collective-permute-done((bf16[4,1024,256]{2,1,0:T(8,128)(2,1)}, bf16[4,1024,256]{2,1,0:T(8,128)(2,1)S(1)}, u32[]{:S(2)}, u32[]{:S(2)}) %collective-permute-start.6) | collective-permute-done | bytes 2097184 | tf_op jit(solution)/shard_map/ppermute | solution.py:28
  213.1 1.6 convolution_bitcast_fusion.3
  214.7 0.0 collective-permute-done.7
  214.7 1.6 convolution_bitcast_fusion
  216.2 2.8 %pad_maximum_fusion.1 = f32[4,384,4,256]{3,1,2,0:T(8,128)} fusion(f32[1,384,4,256]{3,1,2,0:T(8,128)S(1)} %convolution_bitcast_fusion, f32[1,384,4,256]{3,1,2,0:T(8,128)S(1)} %convolution_bitcast_fusion.1, f32[1,384,4,256]{3,1,2,0:T(8,128)S(1)} %convolution_bitcast_fusion.2, f32[1,384,4,256]{3,1,2,0:T(8,128)S(1)} %convolution_bitcast_fusion.3), kind=kLoop, calls=%fused_computation.9 | loop fusion | flops 4718592 | bytes 12582912 | tf_op jit(solution)/shard_map/stack | solution.py:36
  219.1 6.3 %gather_fusion.1 = f32[4,384,4,256]{3,1,2,0:T(8,128)} fusion(f32[4,384,4,256]{3,1,2,0:T(8,128)} %pad_maximum_fusion.1, s32[1024]{0:T(1024)S(1)} %pad_clamp_fusion), kind=kCustom, calls=%fused_computation.1 | custom fusion | bytes 12582928 | tf_op jit(solution)/shard_map/gather | solution.py:37
  225.4 9.4 %copy.6 = f32[384,4,4,256]{3,2,1,0:T(4,128)} copy(f32[384,4,4,256]{3,0,1,2:T(8,128)} %bitcast.68) | data formatting | bytes 12582912 | tf_op jit(solution)/shard_map/transpose | solution.py:17
  234.9 8.3 %reshape_reshape.7 = f32[384,4096]{1,0:T(8,128)} reshape(f32[384,4,4,256]{3,2,1,0:T(4,128)} %copy.6) | data formatting | bytes 12582912 | tf_op jit(solution)/shard_map/reshape;reshape | solution.py:82
  243.1 8.0 %add_convert_fusion = bf16[384,4096]{1,0:T(8,128)(2,1)} fusion(f32[384,4096]{1,0:T(8,128)} %reshape_reshape.7, f32[4096]{0:T(1024)S(1)} %bitcast.73, f32[384,4096]{1,0:T(8,128)} %reshape_reshape.6, f32[4096]{0:T(1024)S(1)} %bitcast.72, bf16[384,4096]{1,0:T(8,128)(2,1)S(1)} %copy-done.1), kind=kLoop, calls=%fused_computation.10 | loop fusion | flops 9437184 | bytes 18907136 | tf_op jit(solution)/shard_map/convert_element_type | solution.py:83
  (17 shorter events, 0.2 us)
Async XLA Ops:
  6.5 47.4 %all-gather.5.cloned.1.call-start = ((), (), s32[]{:S(2)}) async-start(), calls=%async_computation | async-start | bytes 2621440 | tf_op jit(solution)/shard_map/all_gather | solution.py:72
  8.8 2.8 %copy-start.7 = (f32[2,4096]{1,0:T(2,128)S(1)}, f32[2,4096]{1,0:T(2,128)}, u32[]{:S(2)}) copy-start(f32[2,4096]{1,0:T(2,128)} %param.5) | copy-start | bytes 98308
  8.8 2.9 %copy-start.1 = (bf16[384,4096]{1,0:T(8,128)(2,1)S(1)}, bf16[384,4096]{1,0:T(8,128)(2,1)}, u32[]{:S(2)}) copy-start(bf16[384,4096]{1,0:T(8,128)(2,1)} %param.4) | copy-start | bytes 9437188
  8.8 93.1 %all-gather.7.cloned.1.call-start = ((), (), s32[]{:S(2)}) async-start(), calls=%async_computation.1 | async-start | bytes 2621440 | tf_op jit(solution)/shard_map/all_gather | solution.py:72
  11.7 6.5 %copy-start.8 = (f32[2,4096]{1,0:T(2,128)S(1)}, f32[2,4096]{1,0:T(2,128)}, u32[]{:S(2)}) copy-start(f32[2,4096]{1,0:T(2,128)} %param.7) | copy-start | bytes 98308
  12.7 1.7 copy-start.2
  14.4 42.6 %collective-permute-start = (bf16[15,4096]{1,0:T(8,128)(2,1)S(1)}, bf16[15,4096]{1,0:T(8,128)(2,1)S(1)}, u32[]{:S(2)}, u32[]{:S(2)}) collective-permute-start(bf16[15,4096]{1,0:T(8,128)(2,1)S(1)} %slice.344), channel_id=1, source_target_pairs={{0,1},{1,2},{2,3},{3,4},{4,5},{5,6},{6,7},{7,8},{8,9},{9,10},{10,1... | collective-permute-start | bytes 368648 | tf_op jit(solution)/shard_map/ppermute | solution.py:44
  54.0 42.2 %collective-permute-start.1 = (bf16[4,1024,256]{2,1,0:T(8,128)(2,1)}, bf16[4,1024,256]{2,1,0:T(8,128)(2,1)}, u32[]{:S(2)}, u32[]{:S(2)}) collective-permute-start(bf16[4,1024,256]{2,1,0:T(8,128)(2,1)} %bitcast.5), channel_id=1, source_target_pairs={{0,1},{1,2},{2,3},{3,0},{4,5},{5,6},{6,7},{7,4},{8,9},{9,10},{10,1... | collective-permute-start | bytes 6291464 | tf_op jit(solution)/shard_map/ppermute | solution.py:28
  63.4 47.6 %collective-permute-start.3 = (bf16[4,1024,256]{2,1,0:T(8,128)(2,1)}, bf16[4,1024,256]{2,1,0:T(8,128)(2,1)}, u32[]{:S(2)}, u32[]{:S(2)}) collective-permute-start(bf16[4,1024,256]{2,1,0:T(8,128)(2,1)} %bitcast.5), channel_id=1, source_target_pairs={{0,3},{1,0},{2,1},{3,2},{4,7},{5,4},{6,5},{7,6},{8,11},{9,8},{10,9... | collective-permute-start | bytes 6291464 | tf_op jit(solution)/shard_map/ppermute | solution.py:30
  96.2 29.0 %collective-permute-start.2 = (bf16[4,1024,256]{2,1,0:T(8,128)(2,1)}, bf16[4,1024,256]{2,1,0:T(8,128)(2,1)}, u32[]{:S(2)}, u32[]{:S(2)}) collective-permute-start(bf16[4,1024,256]{2,1,0:T(8,128)(2,1)} %collective-permute-done.1), channel_id=1, source_target_pairs={{0,1},{1,2},{2,3},{3,0},{4,5},{5,6},{6,7},{7,4},{8,9},{9,10},{10,1... | collective-permute-start | bytes 6291464 | tf_op jit(solution)/shard_map/ppermute | solution.py:28
  101.9 64.3 %collective-permute-start.5 = (bf16[4,1024,256]{2,1,0:T(8,128)(2,1)}, bf16[4,1024,256]{2,1,0:T(8,128)(2,1)}, u32[]{:S(2)}, u32[]{:S(2)}) collective-permute-start(bf16[4,1024,256]{2,1,0:T(8,128)(2,1)} %bitcast.76), channel_id=1, source_target_pairs={{0,1},{1,2},{2,3},{3,0},{4,5},{5,6},{6,7},{7,4},{8,9},{9,10},{10,1... | collective-permute-start | bytes 6291464 | tf_op jit(solution)/shard_map/ppermute | solution.py:28
  103.8 3.6 %copy-start.3 = (bf16[384,1,1024]{2,0,1:T(8,128)(2,1)S(1)}, bf16[384,1,1024]{2,0,1:T(8,128)(2,1)}, u32[]{:S(2)}) copy-start(bf16[384,1,1024]{2,0,1:T(8,128)(2,1)} %fusion.34) | copy-start | bytes 2359300
  103.8 3.6 %copy-start.4 = (bf16[384,1,1024]{2,0,1:T(8,128)(2,1)S(1)}, bf16[384,1,1024]{2,0,1:T(8,128)(2,1)}, u32[]{:S(2)}) copy-start(bf16[384,1,1024]{2,0,1:T(8,128)(2,1)} %get-tuple-element.8) | copy-start | bytes 2359300
  103.8 3.7 %copy-start.5 = (bf16[384,1,1024]{2,0,1:T(8,128)(2,1)S(1)}, bf16[384,1,1024]{2,0,1:T(8,128)(2,1)}, u32[]{:S(2)}) copy-start(bf16[384,1,1024]{2,0,1:T(8,128)(2,1)} %get-tuple-element.9) | copy-start | bytes 2359300
  103.8 3.7 %copy-start.6 = (bf16[384,1,1024]{2,0,1:T(8,128)(2,1)S(1)}, bf16[384,1,1024]{2,0,1:T(8,128)(2,1)}, u32[]{:S(2)}) copy-start(bf16[384,1,1024]{2,0,1:T(8,128)(2,1)} %get-tuple-element.10) | copy-start | bytes 2359300
  155.6 4.6 %copy-start = (f32[384,4096]{1,0:T(8,128)S(1)}, f32[384,4096]{1,0:T(8,128)}, u32[]{:S(2)}) copy-start(f32[384,4096]{1,0:T(8,128)} %reshape_reshape.6) | copy-start | bytes 18874372
  160.2 6.0 %copy-start.9 = (bf16[1,4,1024,256]{3,2,1,0:T(8,128)(2,1)S(1)}, bf16[1,4,1024,256]{3,2,1,0:T(8,128)(2,1)}, u32[]{:S(2)}) copy-start(bf16[1,4,1024,256]{3,2,1,0:T(8,128)(2,1)} %all-gather.7.cloned.1.call-done) | copy-start | bytes 6291460
  161.8 6.3 %collective-permute-start.4 = (bf16[15,4096]{1,0:T(8,128)(2,1)S(1)}, bf16[15,4096]{1,0:T(8,128)(2,1)S(1)}, u32[]{:S(2)}, u32[]{:S(2)}) collective-permute-start(bf16[15,4096]{1,0:T(8,128)(2,1)S(1)} %slice.375), channel_id=1, source_target_pairs={{0,1},{1,2},{2,3},{3,4},{4,5},{5,6},{6,7},{7,8},{8,9},{9,10},{10,1... | collective-permute-start | bytes 368648 | tf_op jit(solution)/shard_map/ppermute | solution.py:44
  166.2 48.5 %collective-permute-start.7 = (bf16[4,1024,256]{2,1,0:T(8,128)(2,1)S(1)}, bf16[4,1024,256]{2,1,0:T(8,128)(2,1)S(1)}, u32[]{:S(2)}, u32[]{:S(2)}) collective-permute-start(bf16[4,1024,256]{2,1,0:T(8,128)(2,1)S(1)} %bitcast.77), channel_id=1, source_target_pairs={{0,3},{1,0},{2,1},{3,2},{4,7},{5,4},{6,5},{7,6},{8,11},{9,8},{10,9... | collective-permute-start | bytes 6291464 | tf_op jit(solution)/shard_map/ppermute | solution.py:30
  166.2 46.9 %collective-permute-start.6 = (bf16[4,1024,256]{2,1,0:T(8,128)(2,1)}, bf16[4,1024,256]{2,1,0:T(8,128)(2,1)S(1)}, u32[]{:S(2)}, u32[]{:S(2)}) collective-permute-start(bf16[4,1024,256]{2,1,0:T(8,128)(2,1)} %collective-permute-done.5), channel_id=1, source_target_pairs={{0,1},{1,2},{2,3},{3,0},{4,5},{5,6},{6,7},{7,4},{8,9},{9,10},{10,1... | collective-permute-start | bytes 6291464 | tf_op jit(solution)/shard_map/ppermute | solution.py:28
Sparse Core Ops, SparseCore 0:
  8.9 44.9 all-gather.4
  55.5 45.9 all-gather.6
